TPU v7x, 32 devices: a whole 2x2x4 slice. The times are simulated.
32 devices in a mesh: fs: 16 (over z, y, x), tp: 2 (over core).
Axes of the slice: x: 2, y: 2, z: 4, core: 2. Of those that a mesh axis runs over, the one named last changes fastest.
Arguments:
- tokens: bfloat16 [2, 256, 2048], P('tp'), may hold values from -6 to 6
- gain_first: float32 [2048], P('fs'), may hold values from 0.1 to 1.9
- gate_first: float32 [2048, 5632], P('fs', 'tp'), may hold values from -0.125 to 0.125
- up_first: float32 [2048, 5632], P('fs', 'tp'), may hold values from -0.125 to 0.125
- down_first: float32 [2048, 5632], P('fs', 'tp'), may hold values from -0.3125 to 0.3125
- gain_second: float32 [2048], P('fs'), may hold values from 0.1 to 1.9
- gate_second: float32 [2048, 5632], P('fs', 'tp'), may hold values from -0.125 to 0.125
- up_second: float32 [2048, 5632], P('fs', 'tp'), may hold values from -0.125 to 0.125
- down_second: float32 [2048, 5632], P('fs', 'tp'), may hold values from -0.3125 to 0.3125
Outputs:
- mixed: bfloat16 [2, 256, 2048], P('tp', 'fs')
- served_gate_first: bfloat16 [2, 2816, 2048], P(None, 'fs')
- served_up_first: bfloat16 [2, 2816, 2048], P(None, 'fs')
- served_down_first: bfloat16 [2, 2816, 2048], P(None, 'fs')
- served_gate_second: bfloat16 [2, 2816, 2048], P(None, 'fs')
- served_up_second: bfloat16 [2, 2816, 2048], P(None, 'fs')
- served_down_second: bfloat16 [2, 2816, 2048], P(None, 'fs')
All inputs are finite; a program needn't handle non-finite values.
Results may differ from a plain program's by a relative error of at most 0.013.
Values may be sent and summed in bfloat16 or wider, within the bound.
A program may use at most 64 MiB of HBM per device.

v0:
```python
import jax
import jax.numpy as jnp
from jax import lax
from jax.sharding import PartitionSpec as P


def normalize(values):
    wide = values.astype(jnp.float32)
    scale = lax.rsqrt(jnp.mean(wide * wide, axis=-1, keepdims=True) + 1e-06)
    return (wide * scale).astype(jnp.bfloat16)


def folded(weight, gain):
    return (weight * gain[:, None]).astype(jnp.bfloat16).T


def relayout(gate_part, up_part, down_part):
    gate_cut, up_cut, down_cut = (
        lax.all_to_all(gate_part, "fs", split_axis=0, concat_axis=1, tiled=True),
        lax.all_to_all(up_part, "fs", split_axis=0, concat_axis=1, tiled=True),
        lax.all_to_all(down_part, "fs", split_axis=0, concat_axis=1, tiled=True),
    )
    return (
        lax.all_gather(gate_cut[None], "tp", axis=0, tiled=True),
        lax.all_gather(up_cut[None], "tp", axis=0, tiled=True),
        lax.all_gather(down_cut[None], "tp", axis=0, tiled=True),
    )


def hidden_of(normed, gate_served, up_served):
    gate_flat = gate_served.reshape(-1, gate_served.shape[2])
    up_flat = up_served.reshape(-1, up_served.shape[2])
    gate_act = jnp.einsum("rd,hd->rh", normed, gate_flat, preferred_element_type=jnp.float32)
    up_act = jnp.einsum("rd,hd->rh", normed, up_flat, preferred_element_type=jnp.float32)
    return (jax.nn.silu(gate_act) * up_act).astype(jnp.bfloat16)


def projector(hidden, down_flat):
    return jnp.dot(hidden, down_flat, preferred_element_type=jnp.float32)


def shards(
    tokens,
    gain_first,
    gate_first,
    up_first,
    down_first,
    gain_second,
    gate_second,
    up_second,
    down_second,
):
    gate_one, up_one, down_one = relayout(
        folded(gate_first, gain_first),
        folded(up_first, gain_first),
        down_first.astype(jnp.bfloat16).T,
    )
    gate_two, up_two, down_two = relayout(
        folded(gate_second, gain_second),
        folded(up_second, gain_second),
        down_second.astype(jnp.bfloat16).T,
    )
    rows = tokens[0]
    keep = rows.shape[0] // lax.axis_size("fs")
    offset = lax.axis_index("fs") * keep
    hidden_first = hidden_of(normalize(rows), gate_one, up_one)
    down_flat_one = down_one.reshape(-1, down_one.shape[2])
    partial_value = jnp.dot(hidden_first, down_flat_one, preferred_element_type=jnp.float32)
    branch = lax.psum(partial_value, "fs")
    whole_middle = (rows.astype(jnp.float32) + 0.5 * branch).astype(jnp.bfloat16)
    hidden_second = hidden_of(normalize(whole_middle), gate_two, up_two)
    middle = lax.dynamic_slice_in_dim(whole_middle, offset, keep, 0)
    down_flat_two = down_two.reshape(-1, down_two.shape[2])
    branch_two = lax.psum_scatter(
        projector(hidden_second, down_flat_two), "fs", scatter_dimension=0, tiled=True
    )
    mixed = (middle.astype(jnp.float32) + 0.5 * branch_two).astype(jnp.bfloat16)[None]
    return (mixed, gate_one, up_one, down_one, gate_two, up_two, down_two)


def solution(mesh):
    return jax.shard_map(
        shards,
        mesh=mesh,
        in_specs=(
            P("tp", None, None),
            P("fs"),
            P("fs", "tp"),
            P("fs", "tp"),
            P("fs", "tp"),
            P("fs"),
            P("fs", "tp"),
            P("fs", "tp"),
            P("fs", "tp"),
        ),
        out_specs=(
            P("tp", "fs", None),
            P(None, "fs", None),
            P(None, "fs", None),
            P(None, "fs", None),
            P(None, "fs", None),
            P(None, "fs", None),
            P(None, "fs", None),
        ),
        check_vma=False,
    )
```

profile of v0, /device:TPU:0, one launch (start us, length us, event | category | flops | bytes accessed | tf_op | source)
XLA Modules:
  0.0 395.1 jit_solution(5311903597791260053)
XLA Ops:
  7.2 1.8 copy.40
  9.0 1.8 copy.42
  11.9 28.1 %all_to_all.96 = bf16[16,176,128]{2,1,0:T(8,128)(2,1)S(1)} all-to-all(bf16[16,176,128]{2,1,0:T(8,128)(2,1)S(1)} %bitcast.56), channel_id=1, replica_groups=mesh['fs'=16,'tp'=2] {'fs'}, dimensions={0} | all-to-all | bytes 1441792 | tf_op jit(solution)/shard_map/all_to_all | solution.py:19
  40.3 1.2 broadcast_in_dim.27
  41.5 22.3 %all_to_all.97 = bf16[16,176,128]{2,1,0:T(8,128)(2,1)S(1)} all-to-all(bf16[16,176,128]{2,1,0:T(8,128)(2,1)S(1)} %bitcast.54), channel_id=1, replica_groups=mesh['fs'=16,'tp'=2] {'fs'}, dimensions={0} | all-to-all | bytes 1441792 | tf_op jit(solution)/shard_map/all_to_all | solution.py:20
  64.0 1.2 broadcast_in_dim.28
  66.0 22.3 %all_to_all.98 = bf16[16,176,128]{2,1,0:T(8,128)(2,1)S(1)} all-to-all(bf16[16,176,128]{2,1,0:T(8,128)(2,1)S(1)} %bitcast.64), channel_id=1, replica_groups=mesh['fs'=16,'tp'=2] {'fs'}, dimensions={0} | all-to-all | bytes 1441792 | tf_op jit(solution)/shard_map/all_to_all | solution.py:21
  88.5 1.2 broadcast_in_dim.29
  90.6 1.8 copy.48
  92.4 1.6 fusion.4
  94.0 2.5 fusion.14
  97.1 5.5 %fusion.10 = f32[256,2048]{1,0:T(8,128)} fusion(bf16[352,2048]{1,0:T(8,128)(2,1)} %bitcast.68, bf16[352,2048]{1,0:T(8,128)(2,1)} %bitcast.67, bf16[1,256,2048]{2,1,0:T(8,128)(2,1)} %param.9, f32[256]{0:T(256)S(1)} %add_rsqrt_fusion.1, f32[256,352]{0,1:T(8,128)S(1)} %fusion.14), kind=kOutput, calls=%fused_computation.20 | convolution fusion | flops 740311040 | bytes 6390784 | tf_op jit(solution)/shard_map/dot_general | solution.py:68
  104.3 41.4 %all_to_all.99 = bf16[16,176,128]{2,1,0:T(8,128)(2,1)S(1)} all-to-all(bf16[16,176,128]{2,1,0:T(8,128)(2,1)S(1)} %bitcast.57), channel_id=1, replica_groups=mesh['fs'=16,'tp'=2] {'fs'}, dimensions={0} | all-to-all | bytes 1441792 | tf_op jit(solution)/shard_map/all_to_all | solution.py:19
  147.2 26.7 %all_to_all.100 = bf16[16,176,128]{2,1,0:T(8,128)(2,1)S(1)} all-to-all(bf16[16,176,128]{2,1,0:T(8,128)(2,1)S(1)} %bitcast.55), channel_id=1, replica_groups=mesh['fs'=16,'tp'=2] {'fs'}, dimensions={0} | all-to-all | bytes 1441792 | tf_op jit(solution)/shard_map/all_to_all | solution.py:20
  176.0 23.5 %all_to_all.101 = bf16[16,176,128]{2,1,0:T(8,128)(2,1)S(1)} all-to-all(bf16[16,176,128]{2,1,0:T(8,128)(2,1)S(1)} %bitcast.65), channel_id=1, replica_groups=mesh['fs'=16,'tp'=2] {'fs'}, dimensions={0} | all-to-all | bytes 1441792 | tf_op jit(solution)/shard_map/all_to_all | solution.py:21
  201.2 50.3 %all-reduce.2.cloned.1.call-done = f32[256,2048]{1,0:T(8,128)} async-done(((f32[256,2048]{1,0:T(8,128)}), f32[256,2048]{1,0:T(8,128)}) %all-reduce.2.cloned.1.call-update) | async-done | bytes 2097168 | tf_op jit(solution)/shard_map/psum | solution.py:69
  251.4 2.1 fusion.2
  253.6 8.7 %all-gather.13.cloned.1.call-done = bf16[2,176,2048]{2,1,0:T(8,128)(2,1)} async-done(((bf16[1,176,2048]{2,1,0:T(8,128)(2,1)}), bf16[2,176,2048]{2,1,0:T(8,128)(2,1)}) %all-gather.13.cloned.1.call-update) | async-done | bytes 1441808 | tf_op jit(solution)/shard_map/all_gather | solution.py:24
  262.3 2.0 fusion.18
  264.3 10.8 %all-gather.15.cloned.1.call-done = bf16[2,176,2048]{2,1,0:T(8,128)(2,1)} async-done(((bf16[1,176,2048]{2,1,0:T(8,128)(2,1)}), bf16[2,176,2048]{2,1,0:T(8,128)(2,1)}) %all-gather.15.cloned.1.call-update) | async-done | bytes 1441808 | tf_op jit(solution)/shard_map/all_gather | solution.py:25
  275.1 12.9 %all-gather.17.cloned.1.call-done = bf16[2,176,2048]{2,1,0:T(8,128)(2,1)} async-done(((bf16[1,176,2048]{2,1,0:T(8,128)(2,1)}), bf16[2,176,2048]{2,1,0:T(8,128)(2,1)}) %all-gather.17.cloned.1.call-update) | async-done | bytes 1441808 | tf_op jit(solution)/shard_map/all_gather | solution.py:26
  288.0 5.2 %fusion.9 = f32[256,2048]{1,0:T(8,128)} fusion(bf16[352,2048]{1,0:T(8,128)(2,1)} %bitcast.71, bf16[352,2048]{1,0:T(8,128)(2,1)} %bitcast.70, bf16[256,2048]{1,0:T(8,128)(2,1)S(1)} %get-tuple-element.8, f32[256]{0:T(256)S(1)} %add_rsqrt_fusion, f32[256,352]{0,1:T(8,128)S(1)} %fusion.18), kind=kOutput, calls=%fused_computation.19 | convolution fusion | flops 740311040 | bytes 6390784 | tf_op jit(solution)/shard_map/dot_general | solution.py:39
  293.3 82.9 %reduce-scatter.2.cloned.1.call-done = f32[16,2048]{1,0:T(8,128)} async-done(((f32[256,2048]{1,0:T(8,128)}), f32[16,2048]{1,0:T(8,128)}) %reduce-scatter.2.cloned.1.call-update) | async-done | bytes 131088 | tf_op jit(solution)/shard_map/reduce_scatter | solution.py:74
  376.2 1.6 fusion.32
  (69 shorter events, 21.4 us)
Async XLA Ops:
  7.2 86.8 %all-gather.7.cloned.1.call-start = ((), (), s32[]{:S(2)}) async-start(), calls=%async_computation.7 | async-start | bytes 2162688 | tf_op jit(solution)/shard_map/all_gather | solution.py:24
  9.0 1.8 copy-start.12
  40.2 1.3 copy-start.1
  41.4 55.1 %all-gather.9.cloned.1.call-start = ((), (), s32[]{:S(2)}) async-start(), calls=%async_computation.8 | async-start | bytes 2162688 | tf_op jit(solution)/shard_map/all_gather | solution.py:25
  64.0 1.6 copy-start.3
  65.2 31.9 %all-gather.11.cloned.1.call-start = ((), (), s32[]{:S(2)}) async-start(), calls=%async_computation.9 | async-start | bytes 2162688 | tf_op jit(solution)/shard_map/all_gather | solution.py:26
  88.5 1.6 copy-start.4
  89.7 161.7 %all-reduce.2.cloned.1.call-start = ((), (), s32[]{:S(2)}) async-start(), calls=%async_computation.10 | async-start | bytes 4194304 | tf_op jit(solution)/shard_map/psum | solution.py:69
  102.6 0.7 copy-start.13
  102.6 159.6 %all-gather.13.cloned.1.call-start = ((), (), s32[]{:S(2)}) async-start(), calls=%async_computation.11 | async-start | bytes 2162688 | tf_op jit(solution)/shard_map/all_gather | solution.py:24
  145.9 1.3 copy-start.2
  147.1 127.9 %all-gather.15.cloned.1.call-start = ((), (), s32[]{:S(2)}) async-start(), calls=%async_computation.12 | async-start | bytes 2162688 | tf_op jit(solution)/shard_map/all_gather | solution.py:25
  174.1 1.6 copy-start.5
  175.3 112.7 %all-gather.17.cloned.1.call-start = ((), (), s32[]{:S(2)}) async-start(), calls=%async_computation.13 | async-start | bytes 2162688 | tf_op jit(solution)/shard_map/all_gather | solution.py:26
  199.7 51.7 %copy-start = (bf16[1,256,2048]{2,1,0:T(8,128)(2,1)S(1)}, bf16[1,256,2048]{2,1,0:T(8,128)(2,1)}, u32[]{:S(2)}) copy-start(bf16[1,256,2048]{2,1,0:T(8,128)(2,1)} %param.9) | copy-start | bytes 3145732
  200.9 175.2 %reduce-scatter.2.cloned.1.call-start = ((), (), s32[]{:S(2)}) async-start(), calls=%async_computation.14 | async-start | bytes 2228224 | tf_op jit(solution)/shard_map/reduce_scatter | solution.py:74
  293.2 84.5 %copy-start.6 = (bf16[2,176,2048]{2,1,0:T(8,128)(2,1)S(1)}, bf16[2,176,2048]{2,1,0:T(8,128)(2,1)}, u32[]{:S(2)}) copy-start(bf16[2,176,2048]{2,1,0:T(8,128)(2,1)} %all-gather.7.cloned.1.call-done) | copy-start | bytes 4325380
  377.7 1.9 copy-start.7
  379.6 1.9 copy-start.8
  381.5 1.9 copy-start.9
  383.4 1.9 copy-start.10
  385.3 1.9 copy-start.11
Sparse Core Ops, SparseCore 0:
  41.6 7.2 all-gather.6
  65.3 7.2 all-gather.8
  89.8 7.2 all-gather.10
  102.8 148.6 all-reduce.1
  253.4 8.8 all-gather.12
  264.3 10.7 all-gather.14
  277.2 10.7 all-gather.16
  293.4 82.7 reduce-scatter.1
where the time goes:
time: 396 us; the launch traced here: 395 us
  waiting for transfers between devices  166 us (42%)
  blocking collectives  164 us (41%)
  local copies, waits for them, and re-layouts  26.9 us (7%)
  matrix products  15.3 us (4%)
  between operations  14.3 us (4%)
  other arithmetic  7.42 us (2%)
    reduce_scatter x1, waiting for transfers between devices, shards(): lax.psum_scatter(projector(hidden_second, down_flat_two), 'fs', scatter_d...  82.9 us
    all_to_all x2, blocking collectives, relayout(): lax.all_to_all(gate_part, 'fs', split_axis=0, concat_axis=1, tiled=True)  69.5 us
    psum x1, waiting for transfers between devices, shards(): branch = lax.psum(partial_value, 'fs')  50.3 us
    all_to_all x2, blocking collectives, relayout(): lax.all_to_all(up_part, 'fs', split_axis=0, concat_axis=1, tiled=True)  49 us
    all_to_all x2, blocking collectives, relayout(): lax.all_to_all(down_part, 'fs', split_axis=0, concat_axis=1, tiled=True)  45.8 us
    unnamed x40, local copies, waits for them, and re-layouts  18.8 us
    all_gather x2, waiting for transfers between devices, relayout(): lax.all_gather(down_cut[None], 'tp', axis=0, tiled=True)  13.5 us
    all_gather x2, waiting for transfers between devices, relayout(): lax.all_gather(up_cut[None], 'tp', axis=0, tiled=True)  10.8 us
  transfers between devices with their start and end apart: 8, of which 6 were waited for; matrix products, arithmetic and copies ran while one was open for 5% of the time, Pallas kernels for 0%

commit v1 on v0

--- a/solution.py
+++ b/solution.py
@@ -66,7 +66,9 @@
     hidden_first = hidden_of(normalize(rows), gate_one, up_one)
     down_flat_one = down_one.reshape(-1, down_one.shape[2])
     partial_value = jnp.dot(hidden_first, down_flat_one, preferred_element_type=jnp.float32)
-    branch = lax.psum(partial_value, "fs")
+    branch = partial_value
+    for hop in (1, 2, 4, 8):
+        branch = branch + lax.ppermute(branch, "fs", [(dev, dev ^ hop) for dev in range(16)])
     whole_middle = (rows.astype(jnp.float32) + 0.5 * branch).astype(jnp.bfloat16)
     hidden_second = hidden_of(normalize(whole_middle), gate_two, up_two)
     middle = lax.dynamic_slice_in_dim(whole_middle, offset, keep, 0)

time: 396 us -> 490 us (1.24)
  waiting for transfers between devices: 166 us -> 228 us
  starting transfers between devices: 0.51 us -> 17.2 us
  other arithmetic: 7.42 us -> 16 us
  blocking collectives: 164 us -> 172 us
    ppermute x0 -> x4, waiting for transfers between devices: none -> 131 us  [shards(): lax.ppermute(branch, 'fs', [(dev, dev ^ hop) for dev in range(16)])]
    all_to_all x2, blocking collectives: 45.8 us -> 121 us  [relayout(): lax.all_to_all(down_part, 'fs', split_axis=0, concat_axis=1, tiled=True)]
    psum x1 -> x0, waiting for transfers between devices: 50.3 us -> none  [shards(): branch = lax.psum(partial_value, 'fs')]
    all_to_all x2 -> x1, blocking collectives: 69.5 us -> 28.1 us  [relayout(): lax.all_to_all(gate_part, 'fs', split_axis=0, concat_axis=1, tiled=True)]
    all_to_all x2 -> x1, blocking collectives: 49 us -> 22.3 us  [relayout(): lax.all_to_all(up_part, 'fs', split_axis=0, concat_axis=1, tiled=True)]
    all_to_all x0 -> x2, starting transfers between devices: none -> 11.3 us  [the longest x1 5.7 us: relayout(): lax.all_to_all(up_part, 'fs', split_axis=0, concat_axis=1, tiled=True)]
    all_gather x2, waiting for transfers between devices: 10.8 us -> 0.04 us  [relayout(): lax.all_gather(up_cut[None], 'tp', axis=0, tiled=True)]
    all_gather x2, waiting for transfers between devices: 8.75 us -> 0.04 us  [relayout(): lax.all_gather(gate_cut[None], 'tp', axis=0, tiled=True)]
  transfers between devices with their start and end apart: 8 -> 13, of which waited for: 6 -> 7; matrix products, arithmetic and copies ran while one was open for 5% -> 6% of each run, Pallas kernels for 0% -> 0%
where the time goes in v1:
time: 490 us; the launch traced here: 489 us
  waiting for transfers between devices  228 us (47%)
  blocking collectives  172 us (35%)
  local copies, waits for them, and re-layouts  28.4 us (6%)
  starting transfers between devices  17.2 us (4%)
  other arithmetic  16 us (3%)
  between operations  14.4 us (3%)
  matrix products  13.2 us (3%)
    ppermute x4, waiting for transfers between devices, shards(): lax.ppermute(branch, 'fs', [(dev, dev ^ hop) for dev in range(16)])  131 us
    all_to_all x2, blocking collectives, relayout(): lax.all_to_all(down_part, 'fs', split_axis=0, concat_axis=1, tiled=True)  121 us
    reduce_scatter x1, waiting for transfers between devices, shards(): lax.psum_scatter(projector(hidden_second, down_flat_two), 'fs', scatter_d...  82.8 us
    all_to_all x1, blocking collectives, relayout(): lax.all_to_all(gate_part, 'fs', split_axis=0, concat_axis=1, tiled=True)  28.1 us
    all_to_all x1, blocking collectives, relayout(): lax.all_to_all(up_part, 'fs', split_axis=0, concat_axis=1, tiled=True)  22.3 us
    unnamed x42, local copies, waits for them, and re-layouts  20.3 us
  transfers between devices with their start and end apart: 13, of which 7 were waited for; matrix products, arithmetic and copies ran while one was open for 6% of the time, Pallas kernels for 0%

profile of v1, /device:TPU:0, one launch (start us, length us, event | category | flops | bytes accessed | tf_op | source)
XLA Modules:
  0.0 488.8 jit_solution(699186305656697307)
XLA Ops:
  11.9 28.1 %all_to_all.96 = bf16[16,176,128]{2,1,0:T(8,128)(2,1)S(1)} all-to-all(bf16[16,176,128]{2,1,0:T(8,128)(2,1)S(1)} %bitcast.56), channel_id=1, replica_groups=mesh['fs'=16,'tp'=2] {'fs'}, dimensions={0} | all-to-all | bytes 1441792 | tf_op jit(solution)/shard_map/all_to_all | solution.py:19
  41.5 22.3 %all_to_all.97 = bf16[16,176,128]{2,1,0:T(8,128)(2,1)S(1)} all-to-all(bf16[16,176,128]{2,1,0:T(8,128)(2,1)S(1)} %bitcast.55), channel_id=1, replica_groups=mesh['fs'=16,'tp'=2] {'fs'}, dimensions={0} | all-to-all | bytes 1441792 | tf_op jit(solution)/shard_map/all_to_all | solution.py:20
  66.0 22.3 %all_to_all.98 = bf16[16,176,128]{2,1,0:T(8,128)(2,1)S(1)} all-to-all(bf16[16,176,128]{2,1,0:T(8,128)(2,1)S(1)} %bitcast.63), channel_id=1, replica_groups=mesh['fs'=16,'tp'=2] {'fs'}, dimensions={0} | all-to-all | bytes 1441792 | tf_op jit(solution)/shard_map/all_to_all | solution.py:21
  90.1 2.0 fusion.12
  92.1 5.0 %all-gather.11.cloned.1.call-done = bf16[2,176,2048]{2,1,0:T(8,128)(2,1)} async-done(((bf16[1,176,2048]{2,1,0:T(8,128)(2,1)}), bf16[2,176,2048]{2,1,0:T(8,128)(2,1)}) %all-gather.11.cloned.1.call-update) | async-done | bytes 1441808 | tf_op jit(solution)/shard_map/all_gather | solution.py:26
  97.1 3.9 fusion.8
  102.8 46.1 %collective-permute-done = f32[256,2048]{1,0:T(8,128)S(1)} collective-permute-done((f32[256,2048]{1,0:T(8,128)S(1)}, f32[256,2048]{1,0:T(8,128)S(1)}, u32[]{:S(2)}, u32[]{:S(2)}) %collective-permute-start) | collective-permute-done | bytes 2097184 | tf_op jit(solution)/shard_map/ppermute | solution.py:71
  148.9 1.9 add.48
  154.4 2.9 copy.48
  157.3 2.7 multiply_convert_fusion.1
  160.0 5.7 %all-to-all-start.4 = ((bf16[16,176,128]{2,1,0:T(8,128)(2,1)}), bf16[16,176,128]{2,1,0:T(8,128)(2,1)S(1)}, u32[]{:S(2)}, u32[]{:S(2)}) async-start(bf16[16,176,128]{2,1,0:T(8,128)(2,1)} %bitcast.54), calls=%async_computation.4 | async-start | bytes 1441792 | tf_op jit(solution)/shard_map/all_to_all | solution.py:20
  165.8 39.4 %collective-permute-done.1 = f32[256,2048]{1,0:T(8,128)} collective-permute-done((f32[256,2048]{1,0:T(8,128)S(1)}, f32[256,2048]{1,0:T(8,128)}, u32[]{:S(2)}, u32[]{:S(2)}) %collective-permute-start.1) | collective-permute-done | bytes 2097184 | tf_op jit(solution)/shard_map/ppermute | solution.py:71
  205.2 2.5 add.49
  207.7 1.8 collective-permute-start.2
  210.9 5.6 %all-to-all-start.3 = ((bf16[16,176,128]{2,1,0:T(8,128)(2,1)}), bf16[16,176,128]{2,1,0:T(8,128)(2,1)S(1)}, u32[]{:S(2)}, u32[]{:S(2)}) async-start(bf16[16,176,128]{2,1,0:T(8,128)(2,1)} %bitcast.15), calls=%async_computation.3 | async-start | bytes 1441792 | tf_op jit(solution)/shard_map/all_to_all | solution.py:19
  216.5 45.6 %collective-permute-done.2 = f32[256,2048]{1,0:T(8,128)} collective-permute-done((f32[256,2048]{1,0:T(8,128)S(1)}, f32[256,2048]{1,0:T(8,128)}, u32[]{:S(2)}, u32[]{:S(2)}) %collective-permute-start.2) | collective-permute-done | bytes 2097184 | tf_op jit(solution)/shard_map/ppermute | solution.py:71
  262.2 3.2 add.50
  265.4 5.5 %all-to-all-done.3 = bf16[16,176,128]{2,1,0:T(8,128)(2,1)S(1)} async-done(((bf16[16,176,128]{2,1,0:T(8,128)(2,1)}), bf16[16,176,128]{2,1,0:T(8,128)(2,1)S(1)}, u32[]{:S(2)}, u32[]{:S(2)}) %all-to-all-start.3) | async-done | bytes 720928 | tf_op jit(solution)/shard_map/all_to_all | solution.py:19
  273.1 98.8 %all_to_all.99 = bf16[16,176,128]{2,1,0:T(8,128)(2,1)S(1)} all-to-all(bf16[16,176,128]{2,1,0:T(8,128)(2,1)S(1)} %bitcast.64), channel_id=1, replica_groups=mesh['fs'=16,'tp'=2] {'fs'}, dimensions={0} | all-to-all | bytes 1441792 | tf_op jit(solution)/shard_map/all_to_all | solution.py:21
  373.6 2.8 fusion.2
  376.4 2.0 fusion.14
  378.4 3.2 all-gather.17.cloned.1.call-done
  381.7 5.3 %fusion.23 = f32[256,2048]{1,0:T(8,128)} fusion(bf16[352,2048]{1,0:T(8,128)(2,1)} %bitcast.70, f32[256,352]{0,1:T(8,128)S(1)} %fusion.14, bf16[352,2048]{1,0:T(8,128)(2,1)} %bitcast.69, bf16[256,2048]{1,0:T(8,128)(2,1)S(1)} %get-tuple-element.8, f32[256]{0:T(256)S(1)} %add_rsqrt_fusion), kind=kOutput, calls=%fused_computation.28 | convolution fusion | flops 740311040 | bytes 6390784 | tf_op jit(solution)/shard_map/dot_general | solution.py:39
  387.0 82.8 %reduce-scatter.2.cloned.1.call-done = f32[16,2048]{1,0:T(8,128)} async-done(((f32[256,2048]{1,0:T(8,128)}), f32[16,2048]{1,0:T(8,128)}) %reduce-scatter.2.cloned.1.call-update) | async-done | bytes 131088 | tf_op jit(solution)/shard_map/reduce_scatter | solution.py:76
  (81 shorter events, 32.7 us)
Async XLA Ops:
  7.2 82.9 %all-gather.7.cloned.1.call-start = ((), (), s32[]{:S(2)}) async-start(), calls=%async_computation.7 | async-start | bytes 2162688 | tf_op jit(solution)/shard_map/all_gather | solution.py:24
  9.0 1.8 copy-start.13
  41.4 50.7 %all-gather.9.cloned.1.call-start = ((), (), s32[]{:S(2)}) async-start(), calls=%async_computation.8 | async-start | bytes 2162688 | tf_op jit(solution)/shard_map/all_gather | solution.py:25
  65.2 31.9 %all-gather.11.cloned.1.call-start = ((), (), s32[]{:S(2)}) async-start(), calls=%async_computation.9 | async-start | bytes 2162688 | tf_op jit(solution)/shard_map/all_gather | solution.py:26
  101.0 1.8 copy-start.4
  101.0 47.9 %collective-permute-start = (f32[256,2048]{1,0:T(8,128)S(1)}, f32[256,2048]{1,0:T(8,128)S(1)}, u32[]{:S(2)}, u32[]{:S(2)}) collective-permute-start(f32[256,2048]{1,0:T(8,128)S(1)} %fusion.8), channel_id=1, source_target_pairs={{0,2},{2,0},{4,6},{6,4},{8,10},{10,8},{12,14},{14,12},{16,18},{18,... | collective-permute-start | bytes 6291464 | tf_op jit(solution)/shard_map/ppermute | solution.py:71
  150.8 3.6 copy-start
  150.8 54.4 %collective-permute-start.1 = (f32[256,2048]{1,0:T(8,128)S(1)}, f32[256,2048]{1,0:T(8,128)}, u32[]{:S(2)}, u32[]{:S(2)}) collective-permute-start(f32[256,2048]{1,0:T(8,128)S(1)} %add.48), channel_id=1, source_target_pairs={{0,4},{2,6},{4,0},{6,2},{8,12},{10,14},{12,8},{14,10},{16,20},{18,... | collective-permute-start | bytes 6291464 | tf_op jit(solution)/shard_map/ppermute | solution.py:71
  154.4 2.9 copy-start.14
  160.0 49.5 %all-to-all-start.4 = ((bf16[16,176,128]{2,1,0:T(8,128)(2,1)}), bf16[16,176,128]{2,1,0:T(8,128)(2,1)S(1)}, u32[]{:S(2)}, u32[]{:S(2)}) async-start(bf16[16,176,128]{2,1,0:T(8,128)(2,1)} %bitcast.54), calls=%async_computation.4 | async-start | bytes 1441792 | tf_op jit(solution)/shard_map/all_to_all | solution.py:20
  165.7 210.7 %all-gather.15.cloned.1.call-start = ((), (), s32[]{:S(2)}) async-start(), calls=%async_computation.11 | async-start | bytes 2162688 | tf_op jit(solution)/shard_map/all_gather | solution.py:25
  207.7 54.5 %collective-permute-start.2 = (f32[256,2048]{1,0:T(8,128)S(1)}, f32[256,2048]{1,0:T(8,128)}, u32[]{:S(2)}, u32[]{:S(2)}) collective-permute-start(f32[256,2048]{1,0:T(8,128)S(1)} %add.49), channel_id=1, source_target_pairs={{0,8},{2,10},{4,12},{6,14},{8,0},{10,2},{12,4},{14,6},{16,24},{18,... | collective-permute-start | bytes 6291464 | tf_op jit(solution)/shard_map/ppermute | solution.py:71
  210.9 60.1 %all-to-all-start.3 = ((bf16[16,176,128]{2,1,0:T(8,128)(2,1)}), bf16[16,176,128]{2,1,0:T(8,128)(2,1)S(1)}, u32[]{:S(2)}, u32[]{:S(2)}) async-start(bf16[16,176,128]{2,1,0:T(8,128)(2,1)} %bitcast.15), calls=%async_computation.3 | async-start | bytes 1441792 | tf_op jit(solution)/shard_map/all_to_all | solution.py:19
  216.5 162.0 %all-gather.13.cloned.1.call-start = ((), (), s32[]{:S(2)}) async-start(), calls=%async_computation.10 | async-start | bytes 2162688 | tf_op jit(solution)/shard_map/all_gather | solution.py:24
  265.4 108.2 %collective-permute-start.3 = (f32[256,2048]{1,0:T(8,128)}, f32[256,2048]{1,0:T(8,128)}, u32[]{:S(2)}, u32[]{:S(2)}) collective-permute-start(f32[256,2048]{1,0:T(8,128)} %add.50), channel_id=1, source_target_pairs={{0,16},{2,18},{4,20},{6,22},{8,24},{10,26},{12,28},{14,30},{16,0},... | collective-permute-start | bytes 6291464 | tf_op jit(solution)/shard_map/ppermute | solution.py:71
  271.1 1.6 copy-start.6
  272.3 109.4 %all-gather.17.cloned.1.call-start = ((), (), s32[]{:S(2)}) async-start(), calls=%async_computation.12 | async-start | bytes 2162688 | tf_op jit(solution)/shard_map/all_gather | solution.py:26
  373.3 96.5 %reduce-scatter.2.cloned.1.call-start = ((), (), s32[]{:S(2)}) async-start(), calls=%async_computation.13 | async-start | bytes 2228224 | tf_op jit(solution)/shard_map/reduce_scatter | solution.py:76
  387.0 84.4 %copy-start.7 = (bf16[2,176,2048]{2,1,0:T(8,128)(2,1)S(1)}, bf16[2,176,2048]{2,1,0:T(8,128)(2,1)}, u32[]{:S(2)}) copy-start(bf16[2,176,2048]{2,1,0:T(8,128)(2,1)} %all-gather.7.cloned.1.call-done) | copy-start | bytes 4325380
  471.4 1.9 copy-start.8
  473.3 1.9 copy-start.9
  475.2 1.9 copy-start.11
  477.1 1.9 copy-start.10
  478.9 1.9 copy-start.12
  (4 other events, 5.5 us)
Sparse Core Ops, SparseCore 0:
  41.6 7.2 all-gather.6
  65.3 7.2 all-gather.8
  89.8 7.2 all-gather.10
  211.0 9.5 all-gather.14
  272.4 7.6 all-gather.12
  373.4 8.2 all-gather.16
  387.1 82.6 reduce-scatter.1
